TPU v7x, 256 devices: a whole 4x4x8 slice. The times are simulated.
256 devices in a mesh: ep: 64 (over z, y, core), tp: 4 (over x).
Axes of the slice: x: 4, y: 4, z: 8, core: 2. Of those that a mesh axis runs over, the one named last changes fastest.
Arguments:
- tokens: bfloat16 [49152, 2048], P('ep', 'tp')
- norm_gain: float32 [2048], P('tp'), may hold values from 0.1 to 1.9
- routing: int32 [49152, 2], P('ep'), may hold values from 0 to 63, as said below
- route_weight: float32 [49152, 2], P('ep'), may hold values from 0.2 to 1
- w_gate: bfloat16 [64, 2048, 512], P('ep', 'tp'), may hold values from -0.125 to 0.125
- w_up: bfloat16 [64, 2048, 512], P('ep', 'tp'), may hold values from -0.125 to 0.125
- w_down: bfloat16 [64, 512, 2048], P('ep', None, 'tp'), may hold values from -0.25 to 0.25
- w_branch_in: bfloat16 [2048, 1024], P('ep', 'tp'), may hold values from -0.125 to 0.125
- w_branch_out: bfloat16 [1024, 2048], P('tp', 'ep'), may hold values from -0.1875 to 0.1875
- branch_gate: float32 [2048], P('tp'), may hold values from -3 to 3
Outputs:
- mixed: bfloat16 [49152, 2048], P('ep', 'tp')
Inputs may be any that keep to these rules, and one draw needn't show every extreme that they name: `routing`: each row names two different experts of the same group; expert e belongs to group e // 16. Among the rows of one device (aligned blocks of 768 rows) no expert is named more than 48 times, and in every block all experts of one group are named exactly 48 times.
All inputs are finite; a program needn't handle non-finite values.
Results may differ from a plain program's by a relative error of at most 0.0069.
Values may be sent and summed in bfloat16 or wider, within the bound.
A program may use at most 128 MiB of HBM per device.

v0:
```python
import jax
import jax.numpy as jnp
from jax import lax
from jax.sharding import PartitionSpec as P

GROUPS = 4
epsilon = 1e-06


def sent_to_all(value, axis):
    size = lax.axis_size(axis)
    return lax.all_to_all(
        jnp.broadcast_to(value[None], (size, *value.shape)), axis, 0, 0, tiled=True
    )


def taken_together(value, axis):
    return sent_to_all(value, axis).sum(axis=0)


def gather_turned(arrays, axis, dims):
    turned = [jnp.moveaxis(a, dim, 0) for a, dim in zip(arrays, dims)]
    both = jnp.concatenate([t.reshape(len(t), -1) for t in turned], axis=1)
    filled, at, gathered = (lax.all_gather(both, axis, axis=0, tiled=True), 0, [])
    for t, dim in zip(turned, dims):
        share = filled[:, at : at + t[0].size].reshape(-1, *t.shape[1:])
        gathered.append(jnp.moveaxis(share, 0, dim))
        at += t[0].size
    return tuple(gathered)


def send_back(result):
    return lax.all_to_all(result, "ep", split_axis=0, concat_axis=0, tiled=True)


def body(
    tokens,
    norm_gain,
    routing,
    route_weight,
    w_gate,
    w_up,
    w_down,
    w_branch_in,
    w_branch_out,
    branch_gate,
):
    token_count, quarter = tokens.shape
    full_width = quarter * lax.axis_size("tp")
    floats = tokens.astype(jnp.float32)
    squares = taken_together(jnp.sum(floats * floats, axis=1), "tp")
    normed = (floats * lax.rsqrt(squares[:, None] / full_width + epsilon) * norm_gain).astype(
        jnp.bfloat16
    )
    expert_count = lax.axis_size("ep") * w_gate.shape[0]
    capacity = token_count // (expert_count // GROUPS)
    flat_ids = routing.reshape(-1)
    one_hot = (flat_ids[:, None] == jnp.arange(expert_count, dtype=jnp.int32)[None, :]).astype(
        jnp.int32
    )
    before = jnp.cumsum(one_hot, axis=0) - one_hot
    position = flat_ids * capacity + jnp.sum(before * one_hot, axis=1)
    copies = jnp.repeat(normed, 2, axis=0)
    buffer = jnp.zeros((expert_count * capacity, quarter), jnp.bfloat16).at[position].set(copies)
    buffer = buffer.reshape(expert_count, capacity, quarter)
    gate_whole, up_whole, down_whole = (
        lax.all_gather(w_gate[0], "tp", axis=0, tiled=True),
        lax.all_gather(w_up[0], "tp", axis=0, tiled=True),
        lax.all_gather(w_down[0], "tp", axis=1, tiled=True),
    )
    row_split = lax.all_to_all(
        lax.all_to_all(buffer, "ep", split_axis=0, concat_axis=0, tiled=True),
        "tp",
        split_axis=0,
        concat_axis=2,
        tiled=True,
    )
    slot_rows = row_split.reshape(-1, row_split.shape[2])
    gate_sum = jnp.dot(slot_rows, gate_whole, preferred_element_type=jnp.float32)
    up_sum = jnp.dot(slot_rows, up_whole, preferred_element_type=jnp.float32)
    hidden = (jax.nn.silu(gate_sum) * up_sum).astype(jnp.bfloat16)
    result = jnp.dot(hidden, down_whole, preferred_element_type=jnp.float32).astype(jnp.bfloat16)
    feature_split = lax.all_to_all(
        result.reshape(row_split.shape), "tp", split_axis=2, concat_axis=0, tiled=True
    )
    returned = send_back(feature_split)
    picked = returned.reshape(expert_count * capacity, quarter)[position].reshape(
        token_count, 2, quarter
    )
    routed = jnp.sum(picked.astype(jnp.float32) * route_weight[:, :, None], axis=1)
    branch_tokens = lax.all_to_all(normed, "tp", split_axis=0, concat_axis=1, tiled=True)
    in_cols, out_rows = gather_turned((w_branch_in, w_branch_out), "tp", (1, 0))
    in_whole, out_whole = gather_turned((in_cols, out_rows), "ep", (0, 1))
    branch_hidden = jax.nn.silu(
        jnp.dot(branch_tokens, in_whole, preferred_element_type=jnp.float32)
    ).astype(jnp.bfloat16)
    branch_local = jnp.dot(branch_hidden, out_whole, preferred_element_type=jnp.float32).astype(
        jnp.bfloat16
    )
    branch = lax.all_to_all(branch_local, "tp", split_axis=1, concat_axis=0, tiled=True)
    return (routed + jax.nn.sigmoid(branch_gate) * branch.astype(jnp.float32)).astype(jnp.bfloat16)


def solution(mesh):
    return jax.shard_map(
        body,
        mesh=mesh,
        in_specs=(
            P("ep", "tp"),
            P("tp"),
            P("ep", None),
            P("ep", None),
            P("ep", "tp", None),
            P("ep", "tp", None),
            P("ep", None, "tp"),
            P("ep", "tp"),
            P("tp", "ep"),
            P("tp"),
        ),
        out_specs=P("ep", "tp"),
        check_vma=False,
    )
```

profile of v0, /device:TPU:2, one launch (start us, length us, event | category | flops | bytes accessed | tf_op | source)
XLA Modules:
  0.0 391.7 jit_solution(14819414351238019944)
XLA Ops:
  6.5 0.7 all-gather.10.cloned.1.call-update
  8.0 1.4 fusion.12
  10.0 5.5 %all-to-all-start = ((f32[4,1,768]{2,1,0:T(1,128)}), f32[4,1,768]{2,1,0:T(1,128)S(1)}, u32[]{:S(2)}, u32[]{:S(2)}) async-start(f32[4,1,768]{2,1,0:T(1,128)} %broadcast_in_dim.7), calls=%async_computation | async-start | bytes 24576 | tf_op jit(solution)/shard_map/all_to_all | solution.py:12
  15.4 0.7 all-gather.14.cloned.1.call-update
  16.9 18.1 %reduce-window.6 = s32[64,12,128]{2,1,0:T(8,128)S(1)} reduce-window(s32[64,12,128]{2,1,0:T(8,128)S(1)} %fusion.27, s32[]{:T(128)} %constant.6.clone.1), window={size=1x1x128 pad=0_0x0_0x127_0}, to_apply=%region_0.0 | reduce-window | flops 12484608 | bytes 786436 | tf_op jit(solution)/shard_map/reduce-window
  36.8 0.9 copy-done
  37.7 0.8 broadcast_in_dim.8
  39.2 9.5 %scatter_custom_fusion = bf16[3072,512]{1,0:T(8,128)(2,1)} fusion(s32[1536]{0:T(1024)S(1)} %fusion.32, bf16[1536,512]{1,0:T(8,128)(2,1)S(1)} %reshape.110, bf16[]{:T(256)} %constant.8.clone.1), kind=kCustom, calls=%fused_computation.23 | custom fusion | bytes 3145730 | tf_op jit(solution)/shard_map/scatter | solution.py:64
  48.7 11.6 %all-to-all-start.1 = ((bf16[64,48,512]{2,1,0:T(8,128)(2,1)}), bf16[64,48,512]{2,1,0:T(8,128)(2,1)S(1)}, u32[]{:S(2)}, u32[]{:S(2)}) async-start(bf16[64,48,512]{2,1,0:T(8,128)(2,1)} %bitcast.74), calls=%async_computation.1 | async-start | bytes 6291456 | tf_op jit(solution)/shard_map/all_to_all | solution.py:72
  60.4 12.7 %all_gather.18 = bf16[1024,64]{0,1:T(8,128)(2,1)S(1)} all-gather(bf16[256,64]{0,1:T(8,128)(2,1)S(1)} %pad_maximum_fusion.1), channel_id=1, replica_groups=mesh['ep'=64,'tp'=4] {'tp'}, dimensions={0}, use_global_device_ids=true | all-gather | bytes 163840 | tf_op jit(solution)/shard_map/all_gather | solution.py:24
  73.7 60.4 %all-to-all-done.1 = bf16[64,48,512]{2,1,0:T(8,128)(2,1)S(1)} async-done(((bf16[64,48,512]{2,1,0:T(8,128)(2,1)}), bf16[64,48,512]{2,1,0:T(8,128)(2,1)S(1)}, u32[]{:S(2)}, u32[]{:S(2)}) %all-to-all-start.1) | async-done | bytes 3145760 | tf_op jit(solution)/shard_map/all_to_all | solution.py:72
  134.2 39.5 %all_to_all.81 = bf16[64,48,512]{2,1,0:T(8,128)(2,1)S(1)} all-to-all(bf16[64,48,512]{2,1,0:T(8,128)(2,1)S(1)} %all-to-all-done.1), channel_id=1, replica_groups=mesh['ep'=64,'tp'=4] {'tp'}, dimensions={0} | all-to-all | bytes 6291456 | tf_op jit(solution)/shard_map/all_to_all | solution.py:71
  173.6 2.6 copy.61
  176.3 1.0 copy.71
  177.3 4.6 %fusion.10 = f32[768,512]{1,0:T(8,128)} fusion(bf16[768,2048]{1,0:T(8,128)(2,1)S(1)} %bitcast.79, bf16[1,2048,512]{2,1,0:T(8,128)(2,1)} %all-gather.10.cloned.1.call-done), kind=kOutput, calls=%fused_computation.12 | convolution fusion | flops 1610612736 | bytes 6815744 | tf_op jit(solution)/shard_map/dot_general | solution.py:79
  182.0 7.9 %convolution_convert_fusion = bf16[768,2048]{1,0:T(8,128)(2,1)} fusion(bf16[1,512,2048]{2,1,0:T(8,128)(2,1)} %all-gather.14.cloned.1.call-done, f32[768,512]{1,0:T(8,128)} %fusion.10, bf16[768,2048]{1,0:T(8,128)(2,1)S(1)} %bitcast.80, bf16[1,2048,512]{2,1,0:T(8,128)(2,1)} %all-gather.12.cloned.1.call-done), kind=kOutput, calls=%fused_computation.6 | convolution fusion | flops 3225157632 | bytes 12058624 | tf_op jit(solution)/shard_map/dot_general | solution.py:82
  189.9 10.5 %copy.62 = bf16[16,48,2048]{1,0,2:T(8,128)(2,1)} copy(bf16[16,48,2048]{2,1,0:T(8,128)(2,1)} %bitcast.82) | data formatting | bytes 6291456 | tf_op jit(solution)/shard_map/reshape | solution.py:84
  200.4 14.8 %reshape.120 = bf16[4,2,196608]{2,1,0:T(2,128)(2,1)} reshape(bf16[2048,16,48]{2,1,0:T(8,128)(2,1)} %bitcast.72) | data formatting | bytes 6291456
  215.2 38.8 %all_to_all.82 = bf16[4,2,196608]{2,1,0:T(2,128)(2,1)S(1)} all-to-all(bf16[4,2,196608]{2,1,0:T(2,128)(2,1)} %reshape.120), channel_id=1, replica_groups=mesh['ep'=64,'tp'=4] {'tp'}, dimensions={0} | all-to-all | bytes 6291456 | tf_op jit(solution)/shard_map/all_to_all | solution.py:83
  254.0 5.6 %all-to-all-start.5 = ((bf16[4,192,512]{2,1,0:T(8,128)(2,1)}), bf16[4,192,512]{2,1,0:T(8,128)(2,1)}, u32[]{:S(2)}, u32[]{:S(2)}) async-start(bf16[4,192,512]{2,1,0:T(8,128)(2,1)} %bitcast.78), calls=%async_computation.5 | async-start | bytes 1572864 | tf_op jit(solution)/shard_map/all_to_all | solution.py:91
  259.6 9.9 %reshape.121 = bf16[2048,16,48]{2,1,0:T(8,128)(2,1)} reshape(bf16[4,2,196608]{2,1,0:T(2,128)(2,1)S(1)} %all_to_all.82) | data formatting | bytes 6291456
  269.5 9.5 %copy.63 = bf16[4,16,48,512]{3,2,1,0:T(8,128)(2,1)} copy(bf16[4,16,48,512]{2,1,3,0:T(8,128)(2,1)} %bitcast.73) | data formatting | bytes 6291456 | tf_op jit(solution)/shard_map/all_to_all | solution.py:83
  279.1 9.2 %all-to-all-start.4 = ((bf16[64,48,512]{2,1,0:T(8,128)(2,1)}), bf16[64,48,512]{2,1,0:T(8,128)(2,1)S(1)}, u32[]{:S(2)}, u32[]{:S(2)}) async-start(bf16[64,48,512]{2,1,0:T(8,128)(2,1)} %bitcast.77), calls=%async_computation.4 | async-start | bytes 6291456 | tf_op jit(solution)/shard_map/all_to_all | solution.py:33
  288.3 2.1 copy.69
  290.4 7.0 %fusion.4 = bf16[192,2048]{1,0:T(8,128)(2,1)} fusion(bf16[2048,2048]{1,0:T(8,128)(2,1)} %all-gather.8.cloned.1.call-done, bf16[192,2048]{1,0:T(8,128)(2,1)} %bitcast.84), kind=kOutput, calls=%fused_computation.8 | convolution fusion | flops 1611988992 | bytes 9961472 | tf_op jit(solution)/shard_map/dot_general | solution.py:97
  297.4 2.1 copy.74
  299.5 62.6 %all-to-all-done.4 = bf16[64,48,512]{2,1,0:T(8,128)(2,1)S(1)} async-done(((bf16[64,48,512]{2,1,0:T(8,128)(2,1)}), bf16[64,48,512]{2,1,0:T(8,128)(2,1)S(1)}, u32[]{:S(2)}, u32[]{:S(2)}) %all-to-all-start.4) | async-done | bytes 3145760 | tf_op jit(solution)/shard_map/all_to_all | solution.py:33
  362.1 4.8 %all-to-all-start.6 = ((bf16[192,4,512]{2,0,1:T(8,128)(2,1)}), bf16[192,4,512]{2,0,1:T(8,128)(2,1)}, u32[]{:S(2)}, u32[]{:S(2)}) async-start(bf16[192,4,512]{2,0,1:T(8,128)(2,1)} %bitcast.81), calls=%async_computation.6 | async-start | bytes 1572864 | tf_op jit(solution)/shard_map/all_to_all | solution.py:100
  367.7 5.4 %gather_fusion = bf16[1536,512]{1,0:T(8,128)(2,1)} fusion(bf16[3072,512]{1,0:T(8,128)(2,1)S(1)} %bitcast.71, s32[2048]{0:T(1024)S(1)} %pad_clamp_fusion), kind=kCustom, calls=%fused_computation | custom fusion | bytes 3151872 | tf_op jit(solution)/shard_map/gather | solution.py:87
  373.1 3.4 reshape.96
  376.5 5.9 %multiply_reduce_fusion = f32[768,512]{1,0:T(8,128)} fusion(f32[768,2,512]{2,1,0:T(2,128)S(1)} %reshape.96, f32[768,2]{1,0:T(8,128)S(1)} %copy.64), kind=kLoop, calls=%fused_computation.7 | loop fusion | flops 1179648 | bytes 4724736 | tf_op jit(solution)/shard_map/reduce_sum | solution.py:90
  382.4 2.7 fusion.16
  (55 shorter events, 6.0 us)
Async XLA Ops:
  6.5 9.6 %copy-start.2 = (s32[768,2]{0,1:T(2,128)S(1)}, s32[768,2]{0,1:T(2,128)}, u32[]{:S(2)}) copy-start(s32[768,2]{0,1:T(2,128)} %param.12) | copy-start | bytes 18436
  6.5 170.8 %all-gather.10.cloned.1.call-start = ((), (), s32[]{:S(2)}) async-start(), calls=%async_computation.8 | async-start | bytes 2621440 | tf_op jit(solution)/shard_map/all_gather | solution.py:67
  7.3 174.7 %all-gather.12.cloned.1.call-start = ((), (), s32[]{:S(2)}) async-start(), calls=%async_computation.9 | async-start | bytes 2621440 | tf_op jit(solution)/shard_map/all_gather | solution.py:68
  10.0 26.5 %all-to-all-start = ((f32[4,1,768]{2,1,0:T(1,128)}), f32[4,1,768]{2,1,0:T(1,128)S(1)}, u32[]{:S(2)}, u32[]{:S(2)}) async-start(f32[4,1,768]{2,1,0:T(1,128)} %broadcast_in_dim.7), calls=%async_computation | async-start | bytes 24576 | tf_op jit(solution)/shard_map/all_to_all | solution.py:12
  15.4 166.5 %all-gather.14.cloned.1.call-start = ((), (), s32[]{:S(2)}) async-start(), calls=%async_computation.10 | async-start | bytes 2621440 | tf_op jit(solution)/shard_map/all_gather | solution.py:69
  35.0 1.6 copy-start.1
  35.0 1.6 copy-start.7
  36.8 0.9 copy-start
  48.7 11.7 %copy-start.3 = (bf16[256,32]{0,1:T(8,128)(2,1)S(1)}, bf16[256,32]{0,1:T(8,128)(2,1)}, u32[]{:S(2)}) copy-start(bf16[256,32]{0,1:T(8,128)(2,1)} %param.18) | copy-start | bytes 49156
  48.7 11.7 %copy-start.4 = (bf16[32,256]{1,0:T(8,128)(2,1)S(1)}, bf16[32,256]{1,0:T(8,128)(2,1)}, u32[]{:S(2)}) copy-start(bf16[32,256]{1,0:T(8,128)(2,1)} %param.17) | copy-start | bytes 49156
  48.7 85.5 %all-to-all-start.1 = ((bf16[64,48,512]{2,1,0:T(8,128)(2,1)}), bf16[64,48,512]{2,1,0:T(8,128)(2,1)S(1)}, u32[]{:S(2)}, u32[]{:S(2)}) async-start(bf16[64,48,512]{2,1,0:T(8,128)(2,1)} %bitcast.74), calls=%async_computation.1 | async-start | bytes 6291456 | tf_op jit(solution)/shard_map/all_to_all | solution.py:72
  60.3 230.1 %all-gather.8.cloned.1.call-start = ((), (), s32[]{:S(2)}) async-start(), calls=%async_computation.7 | async-start | bytes 8519680 | tf_op jit(solution)/shard_map/all_gather | solution.py:24
  254.0 25.0 %all-to-all-start.5 = ((bf16[4,192,512]{2,1,0:T(8,128)(2,1)}), bf16[4,192,512]{2,1,0:T(8,128)(2,1)}, u32[]{:S(2)}, u32[]{:S(2)}) async-start(bf16[4,192,512]{2,1,0:T(8,128)(2,1)} %bitcast.78), calls=%async_computation.5 | async-start | bytes 1572864 | tf_op jit(solution)/shard_map/all_to_all | solution.py:91
  279.1 83.1 %all-to-all-start.4 = ((bf16[64,48,512]{2,1,0:T(8,128)(2,1)}), bf16[64,48,512]{2,1,0:T(8,128)(2,1)S(1)}, u32[]{:S(2)}, u32[]{:S(2)}) async-start(bf16[64,48,512]{2,1,0:T(8,128)(2,1)} %bitcast.77), calls=%async_computation.4 | async-start | bytes 6291456 | tf_op jit(solution)/shard_map/all_to_all | solution.py:33
  297.4 69.5 %copy-start.8 = (f32[512]{0:T(512)S(1)}, f32[512]{0:T(512)}, u32[]{:S(2)}) copy-start(f32[512]{0:T(512)} %param.19) | copy-start | bytes 6148
  297.4 70.1 %copy-start.6 = (f32[768,2]{0,1:T(2,128)S(1)}, f32[768,2]{0,1:T(2,128)}, u32[]{:S(2)}) copy-start(f32[768,2]{0,1:T(2,128)} %param.13) | copy-start | bytes 18436
  362.1 20.3 %all-to-all-start.6 = ((bf16[192,4,512]{2,0,1:T(8,128)(2,1)}), bf16[192,4,512]{2,0,1:T(8,128)(2,1)}, u32[]{:S(2)}, u32[]{:S(2)}) async-start(bf16[192,4,512]{2,0,1:T(8,128)(2,1)} %bitcast.81), calls=%async_computation.6 | async-start | bytes 1572864 | tf_op jit(solution)/shard_map/all_to_all | solution.py:100
  376.5 5.9 %copy-start.5 = (f32[512]{0:T(512)S(1)}, f32[512]{0:T(512)}, u32[]{:S(2)}) copy-start(f32[512]{0:T(512)} %add_divide_fusion) | copy-start | bytes 6148
Sparse Core Ops, SparseCore 0:
  9.1 35.3 all-gather.9
  46.3 34.3 all-gather.11
  82.6 33.3 all-gather.13
  118.6 83.9 all-gather.7
where the time goes:
time: 393 us; the launch traced here: 392 us
  waiting for transfers between devices  125 us (32%)
  blocking collectives  91 us (23%)
  local copies, waits for them, and re-layouts  75.8 us (19%)
  starting transfers between devices  36.7 us (9%)
  other arithmetic  30.1 us (8%)
  matrix products  19.5 us (5%)
  between operations  13.4 us (3%)
    all_to_all x1, waiting for transfers between devices, send_back(): return lax.all_to_all(result, 'ep', split_axis=0, concat_axis=0, tiled=True)  62.6 us
    all_to_all x1, waiting for transfers between devices, body(): lax.all_to_all(buffer, 'ep', split_axis=0, concat_axis=0, tiled=True)  60.4 us
    all_to_all x1, blocking collectives, body(): lax.all_to_all(lax.all_to_all(buffer, 'ep', split_axis=0, concat_axis=0,...  39.5 us
    all_to_all x1, blocking collectives, body(): lax.all_to_all(result.reshape(row_split.shape), 'tp', split_axis=2, conca...  38.8 us
    unnamed x23, local copies, waits for them, and re-layouts  27 us
    another operation x3, other arithmetic  18.4 us
    all_gather x1, blocking collectives, gather_turned(): lax.all_gather(both, axis, axis=0, tiled=True)  12.7 us
    all_to_all x1, starting transfers between devices, body(): lax.all_to_all(buffer, 'ep', split_axis=0, concat_axis=0, tiled=True)  11.6 us
  transfers between devices with their start and end apart: 9, of which 2 were waited for; matrix products, arithmetic and copies ran while one was open for 31% of the time, Pallas kernels for 0%

commit v1 on v0

--- a/solution.py
+++ b/solution.py
@@ -5,6 +5,22 @@
 
 GROUPS = 4
 epsilon = 1e-06
+
+
+def exchange_in_pairs(x, axis, split, join):
+    ways, here = (lax.axis_size(axis), lax.axis_index(axis))
+    width = x.shape[split] // ways
+    dims = list(x.shape)
+    dims[split] = width
+    height = dims[join]
+    dims[join] = height * ways
+    full = jnp.zeros(dims, x.dtype)
+    for mask in range(ways):
+        part = lax.dynamic_slice_in_dim(x, (here ^ mask) * width, width, axis=split)
+        if mask:
+            part = lax.ppermute(part, axis, [(d, d ^ mask) for d in range(ways)])
+        full = lax.dynamic_update_slice_in_dim(full, part, (here ^ mask) * height, axis=join)
+    return full
 
 
 def sent_to_all(value, axis):
@@ -80,9 +96,7 @@
     up_sum = jnp.dot(slot_rows, up_whole, preferred_element_type=jnp.float32)
     hidden = (jax.nn.silu(gate_sum) * up_sum).astype(jnp.bfloat16)
     result = jnp.dot(hidden, down_whole, preferred_element_type=jnp.float32).astype(jnp.bfloat16)
-    feature_split = lax.all_to_all(
-        result.reshape(row_split.shape), "tp", split_axis=2, concat_axis=0, tiled=True
-    )
+    feature_split = exchange_in_pairs(result.reshape(row_split.shape), "tp", 2, 0)
     returned = send_back(feature_split)
     picked = returned.reshape(expert_count * capacity, quarter)[position].reshape(
         token_count, 2, quarter

time: 393 us -> 367 us (0.934)
  blocking collectives: 91 us -> 12.6 us
  waiting for transfers between devices: 125 us -> 202 us
  local copies, waits for them, and re-layouts: 75.8 us -> 39.7 us
  starting transfers between devices: 36.7 us -> 50.1 us
    all_to_all x2 -> x0, blocking collectives: 78.3 us -> none  [the longest x1 39.5 us: body(): lax.all_to_all(lax.all_to_all(buffer, 'ep', split_axis=0, concat_axis=0,...]
    all_to_all x0 -> x1, waiting for transfers between devices: none -> 34.6 us  [body(): lax.all_to_all(lax.all_to_all(buffer, 'ep', split_axis=0, concat_axis=0,...]
    ppermute x0 -> x3, waiting for transfers between devices: none -> 26.7 us  [exchange_in_pairs(): part = lax.ppermute(part, axis, [(d, d ^ mask) for d in range(ways)])]
    unnamed x23 -> x25, local copies, waits for them, and re-layouts: 27 us -> 5.53 us
    all_to_all x1, waiting for transfers between devices: 60.4 us -> 74.7 us  [body(): lax.all_to_all(buffer, 'ep', split_axis=0, concat_axis=0, tiled=True)]
    reshape x1 -> x0, local copies, waits for them, and re-layouts: 10.5 us -> none  [body(): result.reshape(row_split.shape)]
    all_to_all x1 -> x0, local copies, waits for them, and re-layouts: 9.54 us -> none  [body(): lax.all_to_all(result.reshape(row_split.shape), 'tp', split_axis=2, conca...]
    all_to_all x0 -> x1, starting transfers between devices: none -> 4.56 us  [body(): lax.all_to_all(lax.all_to_all(buffer, 'ep', split_axis=0, concat_axis=0,...]
  transfers between devices with their start and end apart: 9 -> 13, of which waited for: 2 -> 7; matrix products, arithmetic and copies ran while one was open for 31% -> 22% of each run, Pallas kernels for 0% -> 0%
where the time goes in v1:
time: 367 us; the launch traced here: 366 us
  waiting for transfers between devices  202 us (55%)
  starting transfers between devices  50.1 us (14%)
  local copies, waits for them, and re-layouts  39.7 us (11%)
  other arithmetic  29.1 us (8%)
  matrix products  19.6 us (5%)
  between operations  13.4 us (4%)
  blocking collectives  12.6 us (3%)
    all_to_all x1, waiting for transfers between devices, body(): lax.all_to_all(buffer, 'ep', split_axis=0, concat_axis=0, tiled=True)  74.7 us
    all_to_all x1, waiting for transfers between devices, send_back(): return lax.all_to_all(result, 'ep', split_axis=0, concat_axis=0, tiled=True)  62.4 us
    all_to_all x1, waiting for transfers between devices, body(): lax.all_to_all(lax.all_to_all(buffer, 'ep', split_axis=0, concat_axis=0,...  34.6 us
    ppermute x3, waiting for transfers between devices, exchange_in_pairs(): part = lax.ppermute(part, axis, [(d, d ^ mask) for d in range(ways)])  26.7 us
    another operation x3, other arithmetic  18.4 us
    all_gather x1, blocking collectives, gather_turned(): lax.all_gather(both, axis, axis=0, tiled=True)  12.6 us
    all_to_all x1, starting transfers between devices, body(): lax.all_to_all(buffer, 'ep', split_axis=0, concat_axis=0, tiled=True)  11.6 us
    all_to_all x1, starting transfers between devices, send_back(): return lax.all_to_all(result, 'ep', split_axis=0, concat_axis=0, tiled=True)  9.61 us
  transfers between devices with their start and end apart: 13, of which 7 were waited for; matrix products, arithmetic and copies ran while one was open for 22% of the time, Pallas kernels for 0%

profile of v1, /device:TPU:2, one launch (start us, length us, event | category | flops | bytes accessed | tf_op | source)
XLA Modules:
  0.0 366.3 jit_solution(14479553542730330553)
XLA Ops:
  9.6 5.5 %all-to-all-start = ((f32[4,1,768]{2,1,0:T(1,128)}), f32[4,1,768]{2,1,0:T(1,128)S(1)}, u32[]{:S(2)}, u32[]{:S(2)}) async-start(f32[4,1,768]{2,1,0:T(1,128)} %broadcast_in_dim.10), calls=%async_computation | async-start | bytes 24576 | tf_op jit(solution)/shard_map/all_to_all | solution.py:28
  16.2 18.1 %reduce-window.6 = s32[64,12,128]{2,1,0:T(8,128)S(1)} reduce-window(s32[64,12,128]{2,1,0:T(8,128)S(1)} %fusion.27, s32[]{:T(128)} %constant.18.clone.1), window={size=1x1x128 pad=0_0x0_0x127_0}, to_apply=%region_0.0 | reduce-window | flops 12484608 | bytes 786436 | tf_op jit(solution)/shard_map/reduce-window
  35.4 12.6 %all_gather.18 = bf16[1024,64]{0,1:T(8,128)(2,1)S(1)} all-gather(bf16[256,64]{0,1:T(8,128)(2,1)S(1)} %pad_maximum_fusion.1), channel_id=1, replica_groups=mesh['ep'=64,'tp'=4] {'tp'}, dimensions={0}, use_global_device_ids=true | all-gather | bytes 163840 | tf_op jit(solution)/shard_map/all_gather | solution.py:40
  50.7 9.5 %scatter_custom_fusion = bf16[3072,512]{1,0:T(8,128)(2,1)} fusion(s32[1536]{0:T(1024)S(1)} %fusion.32, bf16[1536,512]{1,0:T(8,128)(2,1)S(1)} %reshape.110, bf16[]{:T(256)} %constant.16.clone.1), kind=kCustom, calls=%fused_computation.23 | custom fusion | bytes 3145730 | tf_op jit(solution)/shard_map/scatter | solution.py:80
  60.2 11.6 %all-to-all-start.1 = ((bf16[64,48,512]{2,1,0:T(8,128)(2,1)}), bf16[64,48,512]{2,1,0:T(8,128)(2,1)}, u32[]{:S(2)}, u32[]{:S(2)}) async-start(bf16[64,48,512]{2,1,0:T(8,128)(2,1)} %bitcast.2), calls=%async_computation.1 | async-start | bytes 6291456 | tf_op jit(solution)/shard_map/all_to_all | solution.py:88
  72.6 74.7 %all-to-all-done.1 = bf16[64,48,512]{2,1,0:T(8,128)(2,1)} async-done(((bf16[64,48,512]{2,1,0:T(8,128)(2,1)}), bf16[64,48,512]{2,1,0:T(8,128)(2,1)}, u32[]{:S(2)}, u32[]{:S(2)}) %all-to-all-start.1) | async-done | bytes 3145760 | tf_op jit(solution)/shard_map/all_to_all | solution.py:88
  147.3 4.6 %all-to-all-start.2 = ((bf16[64,48,512]{2,1,0:T(8,128)(2,1)}), bf16[64,48,512]{2,1,0:T(8,128)(2,1)S(1)}, u32[]{:S(2)}, u32[]{:S(2)}) async-start(bf16[64,48,512]{2,1,0:T(8,128)(2,1)} %all-to-all-done.1), calls=%async_computation.2 | async-start | bytes 6291456 | tf_op jit(solution)/shard_map/all_to_all | solution.py:87
  151.8 34.6 %all-to-all-done.2 = bf16[64,48,512]{2,1,0:T(8,128)(2,1)S(1)} async-done(((bf16[64,48,512]{2,1,0:T(8,128)(2,1)}), bf16[64,48,512]{2,1,0:T(8,128)(2,1)S(1)}, u32[]{:S(2)}, u32[]{:S(2)}) %all-to-all-start.2) | async-done | bytes 3145760 | tf_op jit(solution)/shard_map/all_to_all | solution.py:87
  186.4 2.6 copy.54
  190.1 4.6 %fusion.10 = f32[768,512]{1,0:T(8,128)} fusion(bf16[768,2048]{1,0:T(8,128)(2,1)S(1)} %bitcast.70, bf16[1,2048,512]{2,1,0:T(8,128)(2,1)} %all-gather.10.cloned.1.call-done), kind=kOutput, calls=%fused_computation.12 | convolution fusion | flops 1610612736 | bytes 6815744 | tf_op jit(solution)/shard_map/dot_general | solution.py:95
  194.8 8.0 %convolution_convert_fusion = bf16[768,2048]{1,0:T(8,128)(2,1)} fusion(bf16[1,512,2048]{2,1,0:T(8,128)(2,1)} %all-gather.14.cloned.1.call-done, f32[768,512]{1,0:T(8,128)} %fusion.10, bf16[768,2048]{1,0:T(8,128)(2,1)S(1)} %bitcast.71, bf16[1,2048,512]{2,1,0:T(8,128)(2,1)} %all-gather.12.cloned.1.call-done), kind=kOutput, calls=%fused_computation.6 | convolution fusion | flops 3225157632 | bytes 12058624 | tf_op jit(solution)/shard_map/dot_general | solution.py:98
  203.1 1.5 copy-done.2
  204.6 1.5 constant_dynamic-slice_fusion
  206.1 1.5 collective-permute-start
  207.7 1.9 collective-permute-start.2
  209.6 6.9 %all-to-all-start.4 = ((bf16[4,192,512]{2,1,0:T(8,128)(2,1)}), bf16[4,192,512]{2,1,0:T(8,128)(2,1)}, u32[]{:S(2)}, u32[]{:S(2)}) async-start(bf16[4,192,512]{2,1,0:T(8,128)(2,1)} %bitcast.68), calls=%async_computation.4 | async-start | bytes 1572864 | tf_op jit(solution)/shard_map/all_to_all | solution.py:105
  216.5 10.4 %collective-permute-done = bf16[16,48,512]{2,1,0:T(8,128)(2,1)} collective-permute-done((bf16[16,48,512]{2,1,0:T(8,128)(2,1)}, bf16[16,48,512]{2,1,0:T(8,128)(2,1)}, u32[]{:S(2)}, u32[]{:S(2)}) %collective-permute-start) | collective-permute-done | bytes 786464 | tf_op jit(solution)/shard_map/ppermute | solution.py:21
  226.9 1.2 constant_dynamic-update-slice_fusion.1
  228.1 15.2 %collective-permute-done.1 = bf16[16,48,512]{2,1,0:T(8,128)(2,1)} collective-permute-done((bf16[16,48,512]{2,1,0:T(8,128)(2,1)}, bf16[16,48,512]{2,1,0:T(8,128)(2,1)}, u32[]{:S(2)}, u32[]{:S(2)}) %collective-permute-start.1) | collective-permute-done | bytes 786464 | tf_op jit(solution)/shard_map/ppermute | solution.py:21
  243.3 1.2 constant_dynamic-update-slice_fusion
  246.8 1.7 copy-done
  248.5 1.3 all-to-all-done.4
  249.8 9.6 %all-to-all-start.3 = ((bf16[64,48,512]{2,1,0:T(8,128)(2,1)}), bf16[64,48,512]{2,1,0:T(8,128)(2,1)S(1)}, u32[]{:S(2)}, u32[]{:S(2)}) async-start(bf16[64,48,512]{2,1,0:T(8,128)(2,1)} %copy-done), calls=%async_computation.3 | async-start | bytes 6291456 | tf_op jit(solution)/shard_map/all_to_all | solution.py:49
  259.4 2.1 copy.60
  261.5 7.0 %fusion.4 = bf16[192,2048]{1,0:T(8,128)(2,1)} fusion(bf16[2048,2048]{1,0:T(8,128)(2,1)} %all-gather.8.cloned.1.call-done, bf16[192,2048]{1,0:T(8,128)(2,1)} %bitcast.74), kind=kOutput, calls=%fused_computation.8 | convolution fusion | flops 1611988992 | bytes 9961472 | tf_op jit(solution)/shard_map/dot_general | solution.py:111
  268.5 2.1 copy.65
  270.6 62.4 %all-to-all-done.3 = bf16[64,48,512]{2,1,0:T(8,128)(2,1)S(1)} async-done(((bf16[64,48,512]{2,1,0:T(8,128)(2,1)}), bf16[64,48,512]{2,1,0:T(8,128)(2,1)S(1)}, u32[]{:S(2)}, u32[]{:S(2)}) %all-to-all-start.3) | async-done | bytes 3145760 | tf_op jit(solution)/shard_map/all_to_all | solution.py:49
  333.0 8.4 %all-to-all-start.5 = ((bf16[192,4,512]{2,0,1:T(8,128)(2,1)}), bf16[192,4,512]{2,0,1:T(8,128)(2,1)}, u32[]{:S(2)}, u32[]{:S(2)}) async-start(bf16[192,4,512]{2,0,1:T(8,128)(2,1)} %bitcast.72), calls=%async_computation.5 | async-start | bytes 1572864 | tf_op jit(solution)/shard_map/all_to_all | solution.py:114
  342.2 5.4 %gather_fusion = bf16[1536,512]{1,0:T(8,128)(2,1)} fusion(bf16[3072,512]{1,0:T(8,128)(2,1)S(1)} %bitcast.65, s32[2048]{0:T(1024)S(1)} %pad_clamp_fusion), kind=kCustom, calls=%fused_computation | custom fusion | bytes 3151872 | tf_op jit(solution)/shard_map/gather | solution.py:101
  347.6 3.4 reshape.96
  351.1 5.9 %multiply_reduce_fusion = f32[768,512]{1,0:T(8,128)} fusion(f32[768,2,512]{2,1,0:T(2,128)S(1)} %reshape.96, f32[768,2]{1,0:T(8,128)S(1)} %copy.55), kind=kLoop, calls=%fused_computation.7 | loop fusion | flops 1179648 | bytes 4724736 | tf_op jit(solution)/shard_map/reduce_sum | solution.py:104
  357.0 2.7 fusion.16
  (66 shorter events, 13.0 us)
Async XLA Ops:
  6.5 2.2 copy-start.3
  6.5 8.5 %copy-start.4 = (s32[768,2]{0,1:T(2,128)S(1)}, s32[768,2]{0,1:T(2,128)}, u32[]{:S(2)}) copy-start(s32[768,2]{0,1:T(2,128)} %param.12) | copy-start | bytes 18436
  6.5 183.6 %all-gather.10.cloned.1.call-start = ((), (), s32[]{:S(2)}) async-start(), calls=%async_computation.7 | async-start | bytes 2621440 | tf_op jit(solution)/shard_map/all_gather | solution.py:83
  7.3 187.5 %all-gather.14.cloned.1.call-start = ((), (), s32[]{:S(2)}) async-start(), calls=%async_computation.9 | async-start | bytes 2621440 | tf_op jit(solution)/shard_map/all_gather | solution.py:85
  8.0 186.8 %all-gather.12.cloned.1.call-start = ((), (), s32[]{:S(2)}) async-start(), calls=%async_computation.8 | async-start | bytes 2621440 | tf_op jit(solution)/shard_map/all_gather | solution.py:84
  9.6 38.5 %all-to-all-start = ((f32[4,1,768]{2,1,0:T(1,128)}), f32[4,1,768]{2,1,0:T(1,128)S(1)}, u32[]{:S(2)}, u32[]{:S(2)}) async-start(f32[4,1,768]{2,1,0:T(1,128)} %broadcast_in_dim.10), calls=%async_computation | async-start | bytes 24576 | tf_op jit(solution)/shard_map/all_to_all | solution.py:28
  15.7 19.3 %copy-start.5 = (bf16[256,32]{0,1:T(8,128)(2,1)S(1)}, bf16[256,32]{0,1:T(8,128)(2,1)}, u32[]{:S(2)}) copy-start(bf16[256,32]{0,1:T(8,128)(2,1)} %param.18) | copy-start | bytes 49156
  15.7 19.3 %copy-start.6 = (bf16[32,256]{1,0:T(8,128)(2,1)S(1)}, bf16[32,256]{1,0:T(8,128)(2,1)}, u32[]{:S(2)}) copy-start(bf16[32,256]{1,0:T(8,128)(2,1)} %param.17) | copy-start | bytes 49156
  16.2 31.9 %copy-start.9 = (f32[512]{0:T(512)S(1)}, f32[512]{0:T(512)}, u32[]{:S(2)}) copy-start(f32[512]{0:T(512)} %param.11) | copy-start | bytes 6148
  48.4 0.9 copy-start.1
  60.2 87.0 %all-to-all-start.1 = ((bf16[64,48,512]{2,1,0:T(8,128)(2,1)}), bf16[64,48,512]{2,1,0:T(8,128)(2,1)}, u32[]{:S(2)}, u32[]{:S(2)}) async-start(bf16[64,48,512]{2,1,0:T(8,128)(2,1)} %bitcast.2), calls=%async_computation.1 | async-start | bytes 6291456 | tf_op jit(solution)/shard_map/all_to_all | solution.py:88
  71.8 189.7 %all-gather.8.cloned.1.call-start = ((), (), s32[]{:S(2)}) async-start(), calls=%async_computation.6 | async-start | bytes 8519680 | tf_op jit(solution)/shard_map/all_gather | solution.py:40
  147.3 39.2 %all-to-all-start.2 = ((bf16[64,48,512]{2,1,0:T(8,128)(2,1)}), bf16[64,48,512]{2,1,0:T(8,128)(2,1)S(1)}, u32[]{:S(2)}, u32[]{:S(2)}) async-start(bf16[64,48,512]{2,1,0:T(8,128)(2,1)} %all-to-all-done.1), calls=%async_computation.2 | async-start | bytes 6291456 | tf_op jit(solution)/shard_map/all_to_all | solution.py:87
  202.7 1.9 copy-start.2
  206.1 20.7 %collective-permute-start = (bf16[16,48,512]{2,1,0:T(8,128)(2,1)}, bf16[16,48,512]{2,1,0:T(8,128)(2,1)}, u32[]{:S(2)}, u32[]{:S(2)}) collective-permute-start(bf16[16,48,512]{2,1,0:T(8,128)(2,1)} %get-tuple-element.7), channel_id=1, source_target_pairs={{0,1},{1,0},{2,3},{3,2},{4,5},{5,4},{6,7},{7,6},{8,9},{9,8},{10,11... | collective-permute-start | bytes 2359304 | tf_op jit(solution)/shard_map/ppermute | solution.py:21
  207.6 35.7 %collective-permute-start.1 = (bf16[16,48,512]{2,1,0:T(8,128)(2,1)}, bf16[16,48,512]{2,1,0:T(8,128)(2,1)}, u32[]{:S(2)}, u32[]{:S(2)}) collective-permute-start(bf16[16,48,512]{2,1,0:T(8,128)(2,1)} %get-tuple-element.6), channel_id=1, source_target_pairs={{0,2},{1,3},{2,0},{3,1},{4,6},{5,7},{6,4},{7,5},{8,10},{9,11},{10,... | collective-permute-start | bytes 2359304 | tf_op jit(solution)/shard_map/ppermute | solution.py:21
  207.7 37.9 %collective-permute-start.2 = (bf16[16,48,512]{2,1,0:T(8,128)(2,1)}, bf16[16,48,512]{2,1,0:T(8,128)(2,1)}, u32[]{:S(2)}, u32[]{:S(2)}) collective-permute-start(bf16[16,48,512]{2,1,0:T(8,128)(2,1)} %get-tuple-element.5), channel_id=1, source_target_pairs={{0,3},{1,2},{2,1},{3,0},{4,7},{5,6},{6,5},{7,4},{8,11},{9,10},{10,... | collective-permute-start | bytes 2359304 | tf_op jit(solution)/shard_map/ppermute | solution.py:21
  209.6 40.2 %all-to-all-start.4 = ((bf16[4,192,512]{2,1,0:T(8,128)(2,1)}), bf16[4,192,512]{2,1,0:T(8,128)(2,1)}, u32[]{:S(2)}, u32[]{:S(2)}) async-start(bf16[4,192,512]{2,1,0:T(8,128)(2,1)} %bitcast.68), calls=%async_computation.4 | async-start | bytes 1572864 | tf_op jit(solution)/shard_map/all_to_all | solution.py:105
  246.8 1.7 copy-start
  249.8 83.3 %all-to-all-start.3 = ((bf16[64,48,512]{2,1,0:T(8,128)(2,1)}), bf16[64,48,512]{2,1,0:T(8,128)(2,1)S(1)}, u32[]{:S(2)}, u32[]{:S(2)}) async-start(bf16[64,48,512]{2,1,0:T(8,128)(2,1)} %copy-done), calls=%async_computation.3 | async-start | bytes 6291456 | tf_op jit(solution)/shard_map/all_to_all | solution.py:49
  268.5 72.9 %copy-start.10 = (f32[512]{0:T(512)S(1)}, f32[512]{0:T(512)}, u32[]{:S(2)}) copy-start(f32[512]{0:T(512)} %param.19) | copy-start | bytes 6148
  268.5 73.5 %copy-start.8 = (f32[768,2]{0,1:T(2,128)S(1)}, f32[768,2]{0,1:T(2,128)}, u32[]{:S(2)}) copy-start(f32[768,2]{0,1:T(2,128)} %param.13) | copy-start | bytes 18436
  333.0 24.0 %all-to-all-start.5 = ((bf16[192,4,512]{2,0,1:T(8,128)(2,1)}), bf16[192,4,512]{2,0,1:T(8,128)(2,1)}, u32[]{:S(2)}, u32[]{:S(2)}) async-start(bf16[192,4,512]{2,0,1:T(8,128)(2,1)} %bitcast.72), calls=%async_computation.5 | async-start | bytes 1572864 | tf_op jit(solution)/shard_map/all_to_all | solution.py:114
  351.1 5.9 %copy-start.7 = (f32[512]{0:T(512)S(1)}, f32[512]{0:T(512)}, u32[]{:S(2)}) copy-start(f32[512]{0:T(512)} %add_divide_fusion) | copy-start | bytes 6148
Sparse Core Ops, SparseCore 0:
  9.1 36.2 all-gather.9
  47.2 33.0 all-gather.13
  82.1 33.3 all-gather.11
  118.1 84.6 all-gather.7
